TPU v7x, 512 devices: a whole 4x8x8 slice. The times are simulated.
512 devices in a mesh: sp: 32 (over z, x), tp: 16 (over y, core).
Axes of the slice: x: 4, y: 8, z: 8, core: 2. Of those that a mesh axis runs over, the one named last changes fastest.
Arguments:
- in_gate: bfloat16 [1024, 8192], P('tp', 'sp'), may hold values from -6 to 6
- out_gate: bfloat16 [1024, 8192], P('tp', 'sp'), may hold values from -6 to 6
- values: bfloat16 [1024, 8192], P('tp', 'sp'), may hold values from -6 to 6
- conv_taps: bfloat16 [3, 1024], P(None, 'tp'), may hold values from -3.5 to 3.5
- doc_ids: int32 [8192], P('sp'), may hold values from 0 to 7, as said below
- residual: bfloat16 [8192, 2048], P('sp'), may hold values from -6 to 6
- out_weight: bfloat16 [1024, 2048], P('tp'), may hold values from -0.1875 to 0.1875
- norm_gain: bfloat16 [2048], replicated, may hold values from 0.099609375 to 1.8984375
- routes: int32 [8192, 2], P('sp'), may hold values from 0 to 31, all different within a row; in each aligned block of 256 rows (0 to 255, 256 to 511, ...) at most 24 rows name the same one
- route_weights: float32 [8192, 2], P('sp'), may hold values from 0.2 to 1
- expert_gate: bfloat16 [32, 2048, 4224], P('sp', None, 'tp'), may hold values from -0.125 to 0.125
- expert_up: bfloat16 [32, 2048, 4224], P('sp', None, 'tp'), may hold values from -0.125 to 0.125
- expert_down: bfloat16 [32, 4224, 2048], P('sp', 'tp'), may hold values from -0.09375 to 0.09375
Outputs:
- merged: bfloat16 [8192, 2048], P('sp', 'tp')
Inputs may be any that keep to these rules, and one draw needn't show every extreme that they name: `routes`: each row names 2 different experts. Within the rows of one index of sp (aligned blocks of 256 rows) no expert is named more than 24 times, a bound that some expert reaches in some blocks. `doc_ids`: never falls along the sequence; starts at 0 and rises by one at each of 7 document starts, each number used.
All inputs are finite; a program needn't handle non-finite values.
Results may differ from a plain program's by a relative error of at most 0.019.
Values may be sent and summed in bfloat16 or wider, within the bound.
A program may use at most 64 MiB of HBM per device.

v0:
```python
import jax
import jax.numpy as jnp
from jax import lax
from jax.sharding import PartitionSpec as P

EPSILON = 1e-06


def shifted(x, axis, by):
    count = lax.axis_size(axis)
    pairs = [(i, i + by) for i in range(count) if 0 <= i + by < count]
    return lax.ppermute(x, axis, pairs)


def in_blocks(x, dim, count):
    before, after = (x.shape[:dim], x.shape[dim + 1 :])
    return jnp.moveaxis(x.reshape(*before, count, -1, *after), dim, 0)


def sum_at_owner(x, axis, dim):
    count = lax.axis_size(axis)
    parts = lax.all_to_all(in_blocks(x, dim, count), axis, 0, 0, tiled=True)
    return jnp.sum(parts.astype(jnp.float32), axis=0)


def copy_for_each(x, axis):
    copies = jnp.broadcast_to(x, (lax.axis_size(axis), *x.shape))
    return lax.all_to_all(copies, axis, split_axis=0, concat_axis=0, tiled=True)


def taken_together(x, axis):
    everything = copy_for_each(x, axis)
    return jnp.sum(everything, axis=0)


def shards(
    in_gate,
    out_gate,
    values,
    conv_taps,
    doc_ids,
    residual,
    out_weight,
    norm_gain,
    routes,
    route_weights,
    expert_gate,
    expert_up,
    expert_down,
):
    gated_in = (in_gate.astype(jnp.float32) * values.astype(jnp.float32)).astype(jnp.bfloat16)
    tail_rows, tail_docs = shifted((gated_in[:, -2:], doc_ids[-2:]), "sp", 1)
    extended = lax.optimization_barrier(jnp.concatenate([tail_rows, gated_in], axis=1)).astype(
        jnp.float32
    )
    docs_ext = jnp.concatenate([tail_docs, doc_ids])
    length = doc_ids.shape[0]
    near_mask = (docs_ext[1 : length + 1] == doc_ids).astype(jnp.float32)
    far_mask = (docs_ext[0:length] == doc_ids).astype(jnp.float32)
    tap_values = conv_taps.astype(jnp.float32)
    convolved = (
        tap_values[2][:, None] * extended[:, 2:]
        + tap_values[1][:, None] * extended[:, 1 : length + 1] * near_mask[None, :]
        + tap_values[0][:, None] * extended[:, 0:length] * far_mask[None, :]
    )
    mixed_rows = (out_gate.astype(jnp.float32) * convolved).astype(jnp.bfloat16)
    partial_value = lax.dot_general(
        mixed_rows, out_weight, (((0,), (0,)), ((), ())), preferred_element_type=jnp.float32
    )
    tp_count = lax.axis_size("tp")
    model_width = residual.shape[1]
    share_width = model_width // tp_count
    column = lax.axis_index("tp") * share_width
    share_sum = sum_at_owner(partial_value.astype(jnp.bfloat16), "tp", 1)
    stream_cols = (
        lax.dynamic_slice_in_dim(residual, column, share_width, 1).astype(jnp.float32) + share_sum
    )
    square_total = taken_together(jnp.sum(stream_cols * stream_cols, axis=1, keepdims=True), "tp")
    inv_rms = lax.rsqrt(square_total / model_width + EPSILON)
    gain_cols = lax.dynamic_slice_in_dim(norm_gain, column, share_width, 0).astype(jnp.float32)
    own_cols = (stream_cols * inv_rms * gain_cols[None, :]).astype(jnp.bfloat16)
    tokens = routes.shape[0]
    top_count = routes.shape[1]
    experts = lax.axis_size("sp")
    capacity = 3 * tokens * top_count // (2 * experts)
    chosen = routes.reshape(-1)
    hits_table = (chosen[:, None] == jnp.arange(experts, dtype=jnp.int32)[None, :]).astype(
        jnp.int32
    )
    earlier = jnp.cumsum(hits_table, axis=0) - hits_table
    ranked = jnp.sum(earlier * hits_table, axis=1)
    slot_index = chosen * capacity + ranked
    owners = jnp.arange(tokens * top_count, dtype=jnp.int32) // top_count
    source = jnp.zeros((experts * capacity,), jnp.int32).at[slot_index].set(owners)
    filled = jnp.zeros((experts * capacity,), jnp.bool_).at[slot_index].set(True)
    gate_weight = expert_gate[0]
    up_weight = expert_up[0]
    down_weight = expert_down[0]
    picked = jnp.where(
        filled[:, None], jnp.take(own_cols, source, axis=0), jnp.zeros((), jnp.bfloat16)
    ).reshape(experts, capacity, share_width)
    arrived = lax.all_to_all(picked, "sp", split_axis=0, concat_axis=0, tiled=True)
    slot_count = arrived.shape[1]
    row_block = arrived.reshape(-1, share_width)
    piece_cols = lax.all_gather(row_block, "tp", axis=1, tiled=True)
    gate_sum = jnp.dot(piece_cols, gate_weight, preferred_element_type=jnp.float32)
    up_sum = jnp.dot(piece_cols, up_weight, preferred_element_type=jnp.float32)
    hidden = (jax.nn.silu(gate_sum) * up_sum).astype(jnp.bfloat16)
    down_sum = jnp.dot(hidden, down_weight, preferred_element_type=jnp.float32)
    summed = lax.psum_scatter(down_sum.astype(jnp.bfloat16), "tp", scatter_dimension=1, tiled=True)
    returned = lax.all_to_all(
        summed.reshape(experts, slot_count, share_width),
        "sp",
        split_axis=0,
        concat_axis=0,
        tiled=True,
    )
    results = jnp.take(returned.reshape(experts * capacity, share_width), slot_index, axis=0)
    results = results.astype(jnp.float32).reshape(tokens, top_count, share_width)
    blended = jnp.sum(route_weights[:, :, None] * results, axis=1)
    return (stream_cols + blended).astype(jnp.bfloat16)


def solution(mesh):
    placed = (
        P("tp", "sp"),
        P("tp", "sp"),
        P("tp", "sp"),
        P(None, "tp"),
        P("sp"),
        P("sp", None),
        P("tp", None),
        P(),
        P("sp", None),
        P("sp", None),
        P("sp", None, "tp"),
        P("sp", None, "tp"),
        P("sp", "tp", None),
    )
    return jax.shard_map(
        shards, mesh=mesh, in_specs=placed, out_specs=P("sp", "tp"), check_vma=False
    )
```

profile of v0, /device:TPU:25, one launch (start us, length us, event | category | flops | bytes accessed | tf_op | source)
XLA Modules:
  0.0 249.2 jit_solution(15345662534989394620)
XLA Ops:
  6.5 0.0 copy-start
  6.5 0.9 multiply_convert_fusion.1
  7.4 0.1 slice.52
  7.5 3.1 %collective-permute-start = (bf16[64,2]{1,0:T(8,128)(2,1)S(1)}, bf16[64,2]{1,0:T(8,128)(2,1)S(1)}, u32[]{:S(2)}, u32[]{:S(2)}) collective-permute-start(bf16[64,2]{1,0:T(8,128)(2,1)S(1)} %slice.52), channel_id=1, source_target_pairs={{0,16},{16,32},{32,48},{48,64},{64,80},{80,96},{96,112},{112,128},... | collective-permute-start | bytes 776 | tf_op jit(solution)/shard_map/ppermute | solution.py:12
  10.6 0.8 slice.41
  11.4 3.1 %collective-permute-start.1 = (s32[2]{0:T(128)S(1)}, s32[2]{0:T(128)S(1)}, u32[]{:S(2)}, u32[]{:S(2)}) collective-permute-start(s32[2]{0:T(128)S(1)} %slice.41), channel_id=1, source_target_pairs={{0,16},{16,32},{32,48},{48,64},{64,80},{80,96},{96,112},{112,128},... | collective-permute-start | bytes 32 | tf_op jit(solution)/shard_map/ppermute | solution.py:12
  14.5 0.7 convert_element_type.64
  15.2 0.0 collective-permute-done.1
  15.2 0.8 pad_add_fusion
  15.9 0.8 compare_convert_fusion.1
  16.7 0.0 collective-permute-done
  16.7 0.1 pad_maximum_fusion
  16.8 1.5 fusion
  18.3 0.0 copy-start.1
  18.3 1.3 copy.41
  19.6 8.7 %all-to-all-start = ((bf16[16,256,128]{2,1,0:T(8,128)(2,1)}), bf16[16,256,128]{2,1,0:T(8,128)(2,1)S(1)}, u32[]{:S(2)}, u32[]{:S(2)}) async-start(bf16[16,256,128]{2,1,0:T(8,128)(2,1)} %bitcast.55), calls=%async_computation | async-start | bytes 2097152 | tf_op jit(solution)/shard_map/all_to_all | solution.py:22
  28.4 0.0 copy-done.1
  28.4 0.1 copy.29
  28.5 0.1 eq.34
  28.6 0.1 reshape.109
  28.8 1.2 reduce-window.6
  30.0 0.2 slice_reduce_fusion
  30.2 0.1 copy.34
  30.4 0.1 mul.131
  30.6 0.1 fusion.14
  30.7 2.4 scatter_custom_fusion.1
  33.2 0.0 copy-start.3
  33.2 21.4 %all-to-all-done = bf16[16,256,128]{2,1,0:T(8,128)(2,1)S(1)} async-done(((bf16[16,256,128]{2,1,0:T(8,128)(2,1)}), bf16[16,256,128]{2,1,0:T(8,128)(2,1)S(1)}, u32[]{:S(2)}, u32[]{:S(2)}) %all-to-all-start) | async-done | bytes 1048608 | tf_op jit(solution)/shard_map/all_to_all | solution.py:22
  54.6 0.1 convert_reduce_fusion
  54.7 1.0 multiply_reduce_fusion.1
  55.7 0.6 broadcast_in_dim.67
  56.3 5.2 %all-to-all-start.1 = ((f32[16,256,1]{1,2,0:T(1,128)}), f32[16,256,1]{1,2,0:T(1,128)S(1)}, u32[]{:S(2)}, u32[]{:S(2)}) async-start(f32[16,256,1]{1,2,0:T(1,128)} %broadcast_in_dim.67), calls=%async_computation.1 | async-start | bytes 32768 | tf_op jit(solution)/shard_map/all_to_all | solution.py:28
  61.5 0.0 all-gather.2.cloned.1.call-start
  61.5 0.8 dynamic-slice_convert_fusion
  62.3 0.1 broadcast_in_dim.65
  62.4 2.4 scatter_custom_fusion
  64.9 0.1 broadcast_in_dim.62
  65.0 1.1 all-to-all-done.1
  66.1 0.9 multiply_convert_fusion
  67.0 1.9 gather_fusion
  68.9 0.3 select_select_fusion
  69.2 25.0 %all_to_all.20 = bf16[32,24,128]{2,1,0:T(8,128)(2,1)} all-to-all(bf16[32,24,128]{2,1,0:T(8,128)(2,1)S(1)} %select_select_fusion), channel_id=1, replica_groups=mesh['sp'=32,'tp'=16] {'sp'}, dimensions={0} | all-to-all | bytes 393216 | tf_op jit(solution)/shard_map/all_to_all | solution.py:102
  94.2 0.0 all-gather.2.cloned.1.call-update
  94.2 0.0 copy-start.4
  94.2 0.0 reduce-scatter.4.cloned.1.call-start
  94.3 41.9 %all-gather.2.cloned.1.call-done = bf16[768,2048]{1,0:T(8,128)(2,1)} async-done(((bf16[768,128]{1,0:T(8,128)(2,1)}), bf16[768,2048]{1,0:T(8,128)(2,1)}) %all-gather.2.cloned.1.call-update) | async-done | bytes 3145744 | tf_op jit(solution)/shard_map/all_gather | solution.py:105
  136.2 0.0 copy-done.3
  136.2 3.8 %fusion.4 = f32[768,264]{0,1:T(8,128)} fusion(bf16[768,2048]{1,0:T(8,128)(2,1)} %all-gather.2.cloned.1.call-done, bf16[1,2048,264]{1,2,0:T(8,128)(2,1)S(1)} %copy-done.3), kind=kOutput, calls=%fused_computation.12 | convolution fusion | flops 830472192 | bytes 5038080 | tf_op jit(solution)/shard_map/dot_general | solution.py:106
  140.0 0.0 copy-done
  140.0 0.0 copy-done.4
  140.0 7.3 %convolution_convert_fusion = bf16[768,2048]{1,0:T(8,128)(2,1)} fusion(bf16[1,264,2048]{2,1,0:T(8,128)(2,1)S(1)} %copy-done, bf16[768,2048]{1,0:T(8,128)(2,1)} %all-gather.2.cloned.1.call-done, bf16[1,2048,264]{1,2,0:T(8,128)(2,1)S(1)} %copy-done.4, f32[768,264]{0,1:T(8,128)} %fusion.4), kind=kOutput, calls=%fused_computation.4 | convolution fusion | flops 1663733760 | bytes 9265152 | tf_op jit(solution)/shard_map/dot_general | solution.py:109
  147.3 4.6 %copy.35 = bf16[768,2048]{0,1:T(8,128)(2,1)} copy(bf16[768,2048]{1,0:T(8,128)(2,1)} %convolution_convert_fusion) | data formatting | bytes 6291456
  151.9 0.0 reduce-scatter.4.cloned.1.call-update
  152.0 64.2 %reduce-scatter.4.cloned.1.call-done = bf16[128,768]{1,0:T(8,128)(2,1)} async-done(((bf16[2048,768]{1,0:T(8,128)(2,1)}), bf16[128,768]{1,0:T(8,128)(2,1)}) %reduce-scatter.4.cloned.1.call-update) | async-done | bytes 196624
  216.1 1.7 copy.36
  217.9 10.1 %all-to-all-start.3 = ((bf16[32,24,128]{2,1,0:T(8,128)(2,1)}), bf16[32,24,128]{2,1,0:T(8,128)(2,1)S(1)}, u32[]{:S(2)}, u32[]{:S(2)}) async-start(bf16[32,24,128]{2,1,0:T(8,128)(2,1)} %bitcast.12), calls=%async_computation.3 | async-start | bytes 393216 | tf_op jit(solution)/shard_map/all_to_all | solution.py:111
  228.0 0.1 reduce_sum.51
  228.1 0.1 copy.32
  228.2 0.2 copy.33
  228.4 0.1 copy.28
  228.6 9.5 %all-to-all-done.3 = bf16[32,24,128]{2,1,0:T(8,128)(2,1)S(1)} async-done(((bf16[32,24,128]{2,1,0:T(8,128)(2,1)}), bf16[32,24,128]{2,1,0:T(8,128)(2,1)S(1)}, u32[]{:S(2)}, u32[]{:S(2)}) %all-to-all-start.3) | async-done | bytes 196640 | tf_op jit(solution)/shard_map/all_to_all | solution.py:111
  238.1 1.3 gather_fusion.1
  239.4 1.5 multiply_reduce_fusion
  240.9 1.5 add_convert_fusion
  (18 shorter events, 0.2 us)
Async XLA Ops:
  6.5 133.5 %copy-start = (bf16[1,264,2048]{2,1,0:T(8,128)(2,1)S(1)}, bf16[1,264,2048]{2,1,0:T(8,128)(2,1)}, u32[]{:S(2)}) copy-start(bf16[1,264,2048]{2,1,0:T(8,128)(2,1)} %param.25) | copy-start | bytes 3244036
  7.5 9.2 %collective-permute-start = (bf16[64,2]{1,0:T(8,128)(2,1)S(1)}, bf16[64,2]{1,0:T(8,128)(2,1)S(1)}, u32[]{:S(2)}, u32[]{:S(2)}) collective-permute-start(bf16[64,2]{1,0:T(8,128)(2,1)S(1)} %slice.52), channel_id=1, source_target_pairs={{0,16},{16,32},{32,48},{48,64},{64,80},{80,96},{96,112},{112,128},... | collective-permute-start | bytes 776 | tf_op jit(solution)/shard_map/ppermute | solution.py:12
  11.4 3.8 %collective-permute-start.1 = (s32[2]{0:T(128)S(1)}, s32[2]{0:T(128)S(1)}, u32[]{:S(2)}, u32[]{:S(2)}) collective-permute-start(s32[2]{0:T(128)S(1)} %slice.41), channel_id=1, source_target_pairs={{0,16},{16,32},{32,48},{48,64},{64,80},{80,96},{96,112},{112,128},... | collective-permute-start | bytes 32 | tf_op jit(solution)/shard_map/ppermute | solution.py:12
  18.3 10.0 %copy-start.1 = (s32[256,2]{0,1:T(2,128)S(1)}, s32[256,2]{0,1:T(2,128)}, u32[]{:S(2)}) copy-start(s32[256,2]{0,1:T(2,128)} %param.21) | copy-start | bytes 6148
  19.6 35.0 %all-to-all-start = ((bf16[16,256,128]{2,1,0:T(8,128)(2,1)}), bf16[16,256,128]{2,1,0:T(8,128)(2,1)S(1)}, u32[]{:S(2)}, u32[]{:S(2)}) async-start(bf16[16,256,128]{2,1,0:T(8,128)(2,1)} %bitcast.55), calls=%async_computation | async-start | bytes 2097152 | tf_op jit(solution)/shard_map/all_to_all | solution.py:22
  33.2 103.0 %copy-start.3 = (bf16[1,2048,264]{1,2,0:T(8,128)(2,1)S(1)}, bf16[1,2048,264]{1,2,0:T(8,128)(2,1)}, u32[]{:S(2)}) copy-start(bf16[1,2048,264]{1,2,0:T(8,128)(2,1)} %param.23) | copy-start | bytes 3244036
  56.3 9.7 %all-to-all-start.1 = ((f32[16,256,1]{1,2,0:T(1,128)}), f32[16,256,1]{1,2,0:T(1,128)S(1)}, u32[]{:S(2)}, u32[]{:S(2)}) async-start(f32[16,256,1]{1,2,0:T(1,128)} %broadcast_in_dim.67), calls=%async_computation.1 | async-start | bytes 32768 | tf_op jit(solution)/shard_map/all_to_all | solution.py:28
  61.5 74.6 %all-gather.2.cloned.1.call-start = ((), (), s32[]{:S(2)}) async-start(), calls=%async_computation.5 | async-start | bytes 3342336 | tf_op jit(solution)/shard_map/all_gather | solution.py:105
  94.2 45.8 %copy-start.4 = (bf16[1,2048,264]{1,2,0:T(8,128)(2,1)S(1)}, bf16[1,2048,264]{1,2,0:T(8,128)(2,1)}, u32[]{:S(2)}) copy-start(bf16[1,2048,264]{1,2,0:T(8,128)(2,1)} %param.24) | copy-start | bytes 3244036
  94.2 121.9 %reduce-scatter.4.cloned.1.call-start = ((), (), s32[]{:S(2)}) async-start(), calls=%async_computation.6 | async-start | bytes 3342336
  151.9 76.5 %copy-start.2 = (f32[256,2]{0,1:T(2,128)S(1)}, f32[256,2]{0,1:T(2,128)}, u32[]{:S(2)}) copy-start(f32[256,2]{0,1:T(2,128)} %param.22) | copy-start | bytes 6148
  217.9 20.2 %all-to-all-start.3 = ((bf16[32,24,128]{2,1,0:T(8,128)(2,1)}), bf16[32,24,128]{2,1,0:T(8,128)(2,1)S(1)}, u32[]{:S(2)}, u32[]{:S(2)}) async-start(bf16[32,24,128]{2,1,0:T(8,128)(2,1)} %bitcast.12), calls=%async_computation.3 | async-start | bytes 393216 | tf_op jit(solution)/shard_map/all_to_all | solution.py:111
Sparse Core Ops, SparseCore 0:
  94.3 41.7 all-gather.1
  152.1 63.9 reduce-scatter.3
where the time goes:
time: 250 us; the launch traced here: 249 us
  waiting for transfers between devices  138 us (55%)
  starting transfers between devices  30.3 us (12%)
  blocking collectives  25 us (10%)
  local copies, waits for them, and re-layouts  18.9 us (8%)
  between operations  13.7 us (5%)
  matrix products  12.7 us (5%)
  other arithmetic  10.6 us (4%)
    unnamed x3, waiting for transfers between devices  64.2 us
    all_gather x1, waiting for transfers between devices, shards(): piece_cols = lax.all_gather(row_block, 'tp', axis=1, tiled=True)  41.9 us
    all_to_all x1, blocking collectives, shards(): lax.all_to_all(picked, 'sp', split_axis=0, concat_axis=0, tiled=True)  25 us
    all_to_all x1, waiting for transfers between devices, sum_at_owner(): parts = lax.all_to_all(in_blocks(x, dim, count), axis, 0, 0, tiled=True)  21.4 us
    all_to_all x1, starting transfers between devices, shards(): lax.all_to_all(summed.reshape(experts, slot_count, share_width), 'sp', sp...  10.1 us
    all_to_all x1, waiting for transfers between devices, shards(): lax.all_to_all(summed.reshape(experts, slot_count, share_width), 'sp', sp...  9.51 us
    all_to_all x1, starting transfers between devices, sum_at_owner(): parts = lax.all_to_all(in_blocks(x, dim, count), axis, 0, 0, tiled=True)  8.75 us
    dot_general x1, matrix products, shards(): down_sum = jnp.dot(hidden, down_weight, preferred_element_type=jnp.float32)  7.29 us
  transfers between devices with their start and end apart: 7, of which 5 were waited for; matrix products, arithmetic and copies ran while one was open for 5% of the time, Pallas kernels for 0%

commit v1 on v0

--- a/solution.py
+++ b/solution.py
@@ -102,7 +102,10 @@
     arrived = lax.all_to_all(picked, "sp", split_axis=0, concat_axis=0, tiled=True)
     slot_count = arrived.shape[1]
     row_block = arrived.reshape(-1, share_width)
-    piece_cols = lax.all_gather(row_block, "tp", axis=1, tiled=True)
+    pass_the_surface = lambda base_x, array_dim: jnp.concatenate(
+        lax.all_to_all(jnp.stack([base_x] * lax.axis_size("tp")), "tp", 0, 0), axis=array_dim
+    )
+    piece_cols = pass_the_surface(row_block, 1)
     gate_sum = jnp.dot(piece_cols, gate_weight, preferred_element_type=jnp.float32)
     up_sum = jnp.dot(piece_cols, up_weight, preferred_element_type=jnp.float32)
     hidden = (jax.nn.silu(gate_sum) * up_sum).astype(jnp.bfloat16)

time: 250 us -> 279 us (1.12)
  blocking collectives: 25 us -> 104 us
  waiting for transfers between devices: 138 us -> 89.1 us
  matrix products: 12.7 us -> 9.51 us
    all_to_all x0 -> x1, blocking collectives: none -> 78.8 us  [shards(): lax.all_to_all(jnp.stack([base_x] * lax.axis_size('tp')), 'tp', 0, 0)]
    all_gather x1 -> x0, waiting for transfers between devices: 41.9 us -> none  [shards(): piece_cols = lax.all_gather(row_block, 'tp', axis=1, tiled=True)]
    unnamed x3 -> x2, waiting for transfers between devices: 64.2 us -> 57.1 us
    dot_general x1, matrix products: 3.84 us -> 1.04 us  [shards(): jnp.dot(piece_cols, gate_weight, preferred_element_type=jnp.float32)]
    unnamed x14 -> x16, local copies, waits for them, and re-layouts: 6.67 us -> 8.59 us
  transfers between devices with their start and end apart: 7 -> 6, of which waited for: 5 -> 4; matrix products, arithmetic and copies ran while one was open for 5% -> 4% of each run, Pallas kernels for 0% -> 0%
where the time goes in v1:
time: 279 us; the launch traced here: 278 us
  blocking collectives  104 us (37%)
  waiting for transfers between devices  89.1 us (32%)
  starting transfers between devices  30.1 us (11%)
  local copies, waits for them, and re-layouts  21.2 us (8%)
  between operations  13.7 us (5%)
  other arithmetic  10.6 us (4%)
  matrix products  9.51 us (3%)
    all_to_all x1, blocking collectives, shards(): lax.all_to_all(jnp.stack([base_x] * lax.axis_size('tp')), 'tp', 0, 0)  78.8 us
    unnamed x2, waiting for transfers between devices  57.1 us
    all_to_all x1, blocking collectives, shards(): lax.all_to_all(picked, 'sp', split_axis=0, concat_axis=0, tiled=True)  24.9 us
    all_to_all x1, waiting for transfers between devices, sum_at_owner(): parts = lax.all_to_all(in_blocks(x, dim, count), axis, 0, 0, tiled=True)  21.4 us
    all_to_all x1, starting transfers between devices, shards(): lax.all_to_all(summed.reshape(experts, slot_count, share_width), 'sp', sp...  9.9 us
    all_to_all x1, waiting for transfers between devices, shards(): lax.all_to_all(summed.reshape(experts, slot_count, share_width), 'sp', sp...  9.55 us
    all_to_all x1, starting transfers between devices, sum_at_owner(): parts = lax.all_to_all(in_blocks(x, dim, count), axis, 0, 0, tiled=True)  8.75 us
    unnamed x16, local copies, waits for them, and re-layouts  8.59 us
  transfers between devices with their start and end apart: 6, of which 4 were waited for; matrix products, arithmetic and copies ran while one was open for 4% of the time, Pallas kernels for 0%

profile of v1, /device:TPU:25, one launch (start us, length us, event | category | flops | bytes accessed | tf_op | source)
XLA Modules:
  0.0 277.9 jit_solution(16135917556823916261)
XLA Ops:
  6.5 0.0 copy-start
  6.5 0.9 multiply_convert_fusion.1
  7.4 0.1 slice.52
  7.5 3.1 %collective-permute-start = (bf16[64,2]{1,0:T(8,128)(2,1)S(1)}, bf16[64,2]{1,0:T(8,128)(2,1)S(1)}, u32[]{:S(2)}, u32[]{:S(2)}) collective-permute-start(bf16[64,2]{1,0:T(8,128)(2,1)S(1)} %slice.52), channel_id=1, source_target_pairs={{0,16},{16,32},{32,48},{48,64},{64,80},{80,96},{96,112},{112,128},... | collective-permute-start | bytes 776 | tf_op jit(solution)/shard_map/ppermute | solution.py:12
  10.6 0.8 slice.41
  11.4 3.1 %collective-permute-start.1 = (s32[2]{0:T(128)S(1)}, s32[2]{0:T(128)S(1)}, u32[]{:S(2)}, u32[]{:S(2)}) collective-permute-start(s32[2]{0:T(128)S(1)} %slice.41), channel_id=1, source_target_pairs={{0,16},{16,32},{32,48},{48,64},{64,80},{80,96},{96,112},{112,128},... | collective-permute-start | bytes 32 | tf_op jit(solution)/shard_map/ppermute | solution.py:12
  14.5 0.7 convert_element_type.64
  15.2 0.0 collective-permute-done.1
  15.2 0.8 pad_add_fusion
  15.9 0.8 compare_convert_fusion.1
  16.7 0.0 collective-permute-done
  16.7 0.1 pad_maximum_fusion
  16.8 1.5 fusion
  18.3 0.0 copy-start.2
  18.3 1.3 copy.44
  19.6 8.7 %all-to-all-start = ((bf16[16,256,128]{2,1,0:T(8,128)(2,1)}), bf16[16,256,128]{2,1,0:T(8,128)(2,1)S(1)}, u32[]{:S(2)}, u32[]{:S(2)}) async-start(bf16[16,256,128]{2,1,0:T(8,128)(2,1)} %bitcast.58), calls=%async_computation | async-start | bytes 2097152 | tf_op jit(solution)/shard_map/all_to_all | solution.py:22
  28.3 0.0 copy-done.2
  28.4 0.1 copy.31
  28.5 0.1 eq.34
  28.6 0.1 reshape.114
  28.8 1.2 reduce-window.6
  30.0 0.2 slice_reduce_fusion
  30.2 0.1 copy.36
  30.4 0.1 mul.131
  30.6 0.1 fusion.11
  30.7 2.4 scatter_custom_fusion.1
  33.2 21.4 %all-to-all-done = bf16[16,256,128]{2,1,0:T(8,128)(2,1)S(1)} async-done(((bf16[16,256,128]{2,1,0:T(8,128)(2,1)}), bf16[16,256,128]{2,1,0:T(8,128)(2,1)S(1)}, u32[]{:S(2)}, u32[]{:S(2)}) %all-to-all-start) | async-done | bytes 1048608 | tf_op jit(solution)/shard_map/all_to_all | solution.py:22
  54.6 0.1 convert_reduce_fusion
  54.7 1.0 multiply_reduce_fusion.1
  55.7 0.6 broadcast_in_dim.67
  56.3 5.2 %all-to-all-start.1 = ((f32[16,256,1]{1,2,0:T(1,128)}), f32[16,256,1]{1,2,0:T(1,128)S(1)}, u32[]{:S(2)}, u32[]{:S(2)}) async-start(f32[16,256,1]{1,2,0:T(1,128)} %broadcast_in_dim.67), calls=%async_computation.1 | async-start | bytes 32768 | tf_op jit(solution)/shard_map/all_to_all | solution.py:28
  61.5 0.0 reduce-scatter.4.cloned.1.call-start
  61.5 0.8 dynamic-slice_convert_fusion
  62.3 0.1 broadcast_in_dim.65
  62.4 2.4 scatter_custom_fusion
  64.9 0.1 broadcast_in_dim.62
  65.0 1.1 all-to-all-done.1
  66.1 0.9 multiply_convert_fusion
  67.0 1.9 gather_fusion
  68.9 0.3 select_select_fusion
  69.2 24.9 %all_to_all.25 = bf16[32,24,128]{2,1,0:T(8,128)(2,1)S(1)} all-to-all(bf16[32,24,128]{2,1,0:T(8,128)(2,1)S(1)} %select_select_fusion), channel_id=1, replica_groups=mesh['sp'=32,'tp'=16] {'sp'}, dimensions={0} | all-to-all | bytes 393216 | tf_op jit(solution)/shard_map/all_to_all | solution.py:102
  94.1 0.1 copy.37
  94.2 0.3 stack.3
  94.5 0.0 copy-start.4
  94.5 78.8 %all_to_all.26 = bf16[16,768,128]{1,2,0:T(8,128)(2,1)S(1)} all-to-all(bf16[16,768,128]{1,2,0:T(8,128)(2,1)S(1)} %stack.3), channel_id=1, replica_groups=mesh['sp'=32,'tp'=16] {'tp'}, dimensions={0} | all-to-all | bytes 6291456 | tf_op jit(solution)/shard_map/all_to_all | solution.py:106
  173.3 1.7 copy-done.1
  175.0 0.0 copy-done.4
  175.0 1.0 fusion.4
  176.1 0.0 copy-done
  176.1 0.2 copy-done.5
  176.3 6.9 %convolution_convert_fusion = bf16[768,2048]{1,0:T(8,128)(2,1)} fusion(bf16[1,264,2048]{2,1,0:T(8,128)(2,1)S(1)} %copy-done, bf16[768,2048]{0,1:T(8,128)(2,1)} %bitcast.62, bf16[1,2048,264]{1,2,0:T(8,128)(2,1)S(1)} %copy-done.5, f32[768,264]{0,1:T(8,128)S(1)} %fusion.4), kind=kOutput, calls=%fused_computation.4 | convolution fusion | flops 1663733760 | bytes 9265152 | tf_op jit(solution)/shard_map/dot_general | solution.py:112
  183.2 4.7 %copy.38 = bf16[768,2048]{0,1:T(8,128)(2,1)} copy(bf16[768,2048]{1,0:T(8,128)(2,1)} %convolution_convert_fusion) | data formatting | bytes 6291456
  187.9 0.0 reduce-scatter.4.cloned.1.call-update
  187.9 57.1 %reduce-scatter.4.cloned.1.call-done = bf16[128,768]{1,0:T(8,128)(2,1)} async-done(((bf16[2048,768]{1,0:T(8,128)(2,1)}), bf16[128,768]{1,0:T(8,128)(2,1)}) %reduce-scatter.4.cloned.1.call-update) | async-done | bytes 196624
  245.0 1.7 copy.39
  246.7 9.9 %all-to-all-start.4 = ((bf16[32,24,128]{2,1,0:T(8,128)(2,1)}), bf16[32,24,128]{2,1,0:T(8,128)(2,1)S(1)}, u32[]{:S(2)}, u32[]{:S(2)}) async-start(bf16[32,24,128]{2,1,0:T(8,128)(2,1)} %bitcast.15), calls=%async_computation.4 | async-start | bytes 393216 | tf_op jit(solution)/shard_map/all_to_all | solution.py:114
  256.6 0.1 reduce_sum.51
  256.8 0.1 copy.34
  256.9 0.2 copy.35
  257.1 0.1 copy.30
  257.2 9.5 %all-to-all-done.4 = bf16[32,24,128]{2,1,0:T(8,128)(2,1)S(1)} async-done(((bf16[32,24,128]{2,1,0:T(8,128)(2,1)}), bf16[32,24,128]{2,1,0:T(8,128)(2,1)S(1)}, u32[]{:S(2)}, u32[]{:S(2)}) %all-to-all-start.4) | async-done | bytes 196640 | tf_op jit(solution)/shard_map/all_to_all | solution.py:114
  266.8 1.3 gather_fusion.1
  268.1 1.5 multiply_reduce_fusion
  269.6 1.5 add_convert_fusion
  (20 shorter events, 0.2 us)
Async XLA Ops:
  6.5 169.6 %copy-start = (bf16[1,264,2048]{2,1,0:T(8,128)(2,1)S(1)}, bf16[1,264,2048]{2,1,0:T(8,128)(2,1)}, u32[]{:S(2)}) copy-start(bf16[1,264,2048]{2,1,0:T(8,128)(2,1)} %param.25) | copy-start | bytes 3244036
  7.5 9.2 %collective-permute-start = (bf16[64,2]{1,0:T(8,128)(2,1)S(1)}, bf16[64,2]{1,0:T(8,128)(2,1)S(1)}, u32[]{:S(2)}, u32[]{:S(2)}) collective-permute-start(bf16[64,2]{1,0:T(8,128)(2,1)S(1)} %slice.52), channel_id=1, source_target_pairs={{0,16},{16,32},{32,48},{48,64},{64,80},{80,96},{96,112},{112,128},... | collective-permute-start | bytes 776 | tf_op jit(solution)/shard_map/ppermute | solution.py:12
  11.4 3.8 %collective-permute-start.1 = (s32[2]{0:T(128)S(1)}, s32[2]{0:T(128)S(1)}, u32[]{:S(2)}, u32[]{:S(2)}) collective-permute-start(s32[2]{0:T(128)S(1)} %slice.41), channel_id=1, source_target_pairs={{0,16},{16,32},{32,48},{48,64},{64,80},{80,96},{96,112},{112,128},... | collective-permute-start | bytes 32 | tf_op jit(solution)/shard_map/ppermute | solution.py:12
  18.3 10.0 %copy-start.2 = (s32[256,2]{0,1:T(2,128)S(1)}, s32[256,2]{0,1:T(2,128)}, u32[]{:S(2)}) copy-start(s32[256,2]{0,1:T(2,128)} %param.21) | copy-start | bytes 6148
  19.6 35.0 %all-to-all-start = ((bf16[16,256,128]{2,1,0:T(8,128)(2,1)}), bf16[16,256,128]{2,1,0:T(8,128)(2,1)S(1)}, u32[]{:S(2)}, u32[]{:S(2)}) async-start(bf16[16,256,128]{2,1,0:T(8,128)(2,1)} %bitcast.58), calls=%async_computation | async-start | bytes 2097152 | tf_op jit(solution)/shard_map/all_to_all | solution.py:22
  56.3 9.7 %all-to-all-start.1 = ((f32[16,256,1]{1,2,0:T(1,128)}), f32[16,256,1]{1,2,0:T(1,128)S(1)}, u32[]{:S(2)}, u32[]{:S(2)}) async-start(f32[16,256,1]{1,2,0:T(1,128)} %broadcast_in_dim.67), calls=%async_computation.1 | async-start | bytes 32768 | tf_op jit(solution)/shard_map/all_to_all | solution.py:28
  61.5 183.5 %reduce-scatter.4.cloned.1.call-start = ((), (), s32[]{:S(2)}) async-start(), calls=%async_computation.6 | async-start | bytes 3342336
  94.5 80.5 %copy-start.4 = (bf16[1,2048,264]{1,2,0:T(8,128)(2,1)S(1)}, bf16[1,2048,264]{1,2,0:T(8,128)(2,1)}, u32[]{:S(2)}) copy-start(bf16[1,2048,264]{1,2,0:T(8,128)(2,1)} %param.23) | copy-start | bytes 3244036
  173.3 1.7 copy-start.1
  175.0 1.2 copy-start.5
  187.9 69.2 %copy-start.3 = (f32[256,2]{0,1:T(2,128)S(1)}, f32[256,2]{0,1:T(2,128)}, u32[]{:S(2)}) copy-start(f32[256,2]{0,1:T(2,128)} %param.22) | copy-start | bytes 6148
  246.7 20.0 %all-to-all-start.4 = ((bf16[32,24,128]{2,1,0:T(8,128)(2,1)}), bf16[32,24,128]{2,1,0:T(8,128)(2,1)S(1)}, u32[]{:S(2)}, u32[]{:S(2)}) async-start(bf16[32,24,128]{2,1,0:T(8,128)(2,1)} %bitcast.15), calls=%async_computation.4 | async-start | bytes 393216 | tf_op jit(solution)/shard_map/all_to_all | solution.py:114
Sparse Core Ops, SparseCore 0:
  188.1 56.8 reduce-scatter.3
